TPU v7x, 32 devices: a whole 2x2x4 slice. The times are simulated.
32 devices in a mesh: gr: 2 (over x), fs: 8 (over z, y), tp: 2 (over core).
Axes of the slice: x: 2, y: 2, z: 4, core: 2. Of those that a mesh axis runs over, the one named last changes fastest.
Arguments:
- tokens: bfloat16 [6144, 2048], P(('gr', 'fs')), may hold values from -6 to 6
- routes: int32 [6144, 4], P(('gr', 'fs')), may hold values from 0 to 7, all different within a row; in each aligned block of 384 rows (0 to 383, 384 to 767, ...) at most 288 rows name the same one
- route_scores: float32 [6144, 4], P(('gr', 'fs')), may hold values from -6 to 6
- norm_gain: float32 [2048], P(('gr', 'fs')), may hold values from 0.1 to 1.9
- gate_master: float32 [8, 2048, 1024], P(None, ('gr', 'fs'), 'tp'), may hold values from -0.875 to 0.875
- up_master: float32 [8, 2048, 1024], P(None, ('gr', 'fs'), 'tp'), may hold values from -0.875 to 0.875
- down_master: float32 [8, 1024, 2048], P(None, ('gr', 'fs'), 'tp'), may hold values from -0.1875 to 0.1875
Outputs:
- gate_weights: bfloat16 [8, 2048, 1024], P('fs', None, 'tp')
- up_weights: bfloat16 [8, 2048, 1024], P('fs', None, 'tp')
- down_weights: bfloat16 [8, 1024, 2048], P('fs', None, 'tp')
- mixed: bfloat16 [6144, 2048], P(('gr', 'fs'), 'tp')
Inputs may be any that keep to these rules, and one draw needn't show every extreme that they name: `routes`: each row names 4 different experts; among the rows of one index of gr+fs no expert is named more than 288 times, a bound that some block reaches.
All inputs are finite; a program needn't handle non-finite values.
Results may differ from a plain program's by a relative error of at most 0.0085.
Values may be sent and summed in bfloat16 or wider, within the bound.
A program may use at most 128 MiB of HBM per device.

v0:
```python
import jax
import jax.numpy as jnp
from jax import lax
from jax.sharding import PartitionSpec as P

NORM_EPS = 1e-05
CLAMP_LIMIT = 7.0
GLU_ALPHA = 1.702


def normalize(tokens):
    values = tokens.astype(jnp.float32)
    centre = jnp.mean(values, -1, keepdims=True)
    spread = jnp.mean(jnp.square(values - centre), -1, keepdims=True)
    return ((values - centre) * lax.rsqrt(spread + NORM_EPS)).astype(jnp.bfloat16)


def reorder(matrix, fs_count, gr_count):
    experts_here, row_count, col_count = matrix.shape
    block_rows = row_count // (fs_count * gr_count)
    shaped = matrix.reshape(experts_here, fs_count, gr_count, block_rows, col_count)
    return jnp.swapaxes(shaped, 1, 2).reshape(experts_here, row_count, col_count)


def per_device(tokens, routes, route_scores, norm_gain, gate_master, up_master, down_master):
    gate_low = (norm_gain[None, :, None] * gate_master).astype(jnp.bfloat16)
    up_low = (norm_gain[None, :, None] * up_master).astype(jnp.bfloat16)
    down_low = down_master.astype(jnp.bfloat16)
    fs_count = lax.axis_size("fs")
    gr_count = lax.axis_size("gr")
    paired = (
        lax.all_gather(gate_low, "gr", axis=1, tiled=True),
        lax.all_gather(up_low, "gr", axis=1, tiled=True),
        lax.all_gather(down_low, "gr", axis=1, tiled=True),
    )
    spread = (
        lax.all_to_all(paired[0], "fs", split_axis=0, concat_axis=1, tiled=True),
        lax.all_to_all(paired[1], "fs", split_axis=0, concat_axis=1, tiled=True),
        lax.all_to_all(paired[2], "fs", split_axis=0, concat_axis=1, tiled=True),
    )
    gate_weights = reorder(spread[0], fs_count, gr_count)
    up_weights = reorder(spread[1], fs_count, gr_count)
    down_weights = reorder(spread[2], fs_count, gr_count)
    tok_count, per_token = routes.shape
    model_width = tokens.shape[1]
    experts = gate_master.shape[0]
    capacity = 3 * tok_count * per_token // (2 * experts)
    normed = normalize(tokens)
    chosen = routes.reshape(-1)
    assigned = tok_count * per_token
    one_hot = (chosen[:, None] == jnp.arange(experts, dtype=jnp.int32)[None, :]).astype(jnp.int32)
    earlier = jnp.cumsum(one_hot, axis=0) - one_hot
    within = jnp.sum(earlier * one_hot, axis=1)
    target = chosen * capacity + within
    anchor = (
        jnp.full((experts * capacity,), assigned, jnp.int32)
        .at[target]
        .set(jnp.arange(assigned, dtype=jnp.int32))
    )
    padded = jnp.concatenate([normed, jnp.zeros((1, model_width), jnp.bfloat16)], axis=0)
    outgoing = padded[anchor // per_token].reshape(experts, capacity, model_width)
    w_gate = gate_weights[0]
    w_up = up_weights[0]
    w_down = down_weights[0]
    share = capacity // lax.axis_size("tp")
    mine = lax.dynamic_slice_in_dim(outgoing, lax.axis_index("tp") * share, share, 1)
    arrived = lax.all_to_all(mine, "fs", split_axis=0, concat_axis=0, tiled=True)
    joined = lax.all_gather(arrived, "tp", axis=1, tiled=True)
    senders, slot_count, width_all = joined.shape
    flat_rows = joined.reshape(senders * slot_count, width_all)
    gate_pre = jnp.minimum(
        jnp.dot(flat_rows, w_gate, preferred_element_type=jnp.float32), CLAMP_LIMIT
    )
    up_pre = jnp.clip(
        jnp.dot(flat_rows, w_up, preferred_element_type=jnp.float32), -CLAMP_LIMIT, CLAMP_LIMIT
    )
    hidden = ((up_pre + 1.0) * gate_pre * jax.nn.sigmoid(GLU_ALPHA * gate_pre)).astype(jnp.bfloat16)
    whole = lax.all_gather(hidden, "tp", axis=1, tiled=True)
    answer = jnp.dot(whole, w_down, preferred_element_type=jnp.float32).astype(jnp.bfloat16)
    answer = answer.reshape(senders, slot_count, answer.shape[1])
    returned = lax.all_to_all(answer, "fs", split_axis=0, concat_axis=0, tiled=True)
    picked = returned.reshape(experts * capacity, returned.shape[2])[target]
    picked = picked.astype(jnp.float32).reshape(tok_count, per_token, returned.shape[2])
    mixing = jax.nn.softmax(route_scores, axis=-1)
    mixed = jnp.sum(picked * mixing[:, :, None], axis=1).astype(jnp.bfloat16)
    return (gate_weights, up_weights, down_weights, mixed)


def solution(mesh):
    in_specs = (
        P(("gr", "fs"), None),
        P(("gr", "fs"), None),
        P(("gr", "fs"), None),
        P(("gr", "fs")),
        P(None, ("gr", "fs"), "tp"),
        P(None, ("gr", "fs"), "tp"),
        P(None, ("gr", "fs"), "tp"),
    )
    out_specs = (
        P("fs", None, "tp"),
        P("fs", None, "tp"),
        P("fs", None, "tp"),
        P(("gr", "fs"), "tp"),
    )
    return jax.shard_map(
        per_device, mesh=mesh, in_specs=in_specs, out_specs=out_specs, check_vma=False
    )
```

profile of v0, /device:TPU:0, one launch (start us, length us, event | category | flops | bytes accessed | tf_op | source)
XLA Modules:
  0.0 470.1 jit_solution(13538109231922596886)
XLA Ops:
  7.2 0.9 copy.19
  8.1 0.1 eq.29
  8.3 0.1 eq.25
  8.4 0.7 broadcast_multiply_fusion
  9.1 2.3 reduce-window.6
  11.4 0.3 slice_reduce_fusion
  11.7 0.2 reduce-window.9
  11.9 0.1 add_bitcast_fusion
  12.0 0.1 copy.18
  12.1 0.2 mul.71
  12.3 6.2 %scatter_custom_fusion = s32[2304]{0:T(1024)S(1)} fusion(s32[1536]{0:T(1024)S(1)} %fusion.10, s32[1536]{0:T(1024)S(1)} %iota.11, s32[]{:T(128)} %constant.25.clone.1), kind=kCustom, calls=%fused_computation.38 | custom fusion | bytes 9220 | tf_op jit(solution)/shard_map/scatter | solution.py:58
  18.6 1.7 convert_reduce_fusion
  20.3 0.6 fusion.2
  20.8 0.5 fusion.3
  21.3 0.2 concatenate.3
  21.5 9.9 %gather_fusion = bf16[2304,2048]{1,0:T(8,128)(2,1)} fusion(bf16[385,2048]{1,0:T(8,128)(2,1)S(1)} %concatenate.3, s32[3072]{0:T(1024)S(1)} %pad_clamp_fusion), kind=kCustom, calls=%fused_computation | custom fusion | bytes 18883584 | tf_op jit(solution)/shard_map/gather | solution.py:61
  31.4 5.2 %constant_dynamic-slice_fusion = bf16[8,144,2048]{2,1,0:T(8,128)(2,1)} fusion(bf16[8,288,2048]{2,1,0:T(8,128)(2,1)} %bitcast.47, s32[]{:T(128)S(6)} %select_n.25), kind=kLoop, calls=%fused_computation.45 | loop fusion | bytes 9437188 | tf_op jit(solution)/shard_map/dynamic_slice | solution.py:66
  36.6 7.4 %all-to-all-start.3 = ((bf16[8,144,2048]{2,1,0:T(8,128)(2,1)}), bf16[8,144,2048]{2,1,0:T(8,128)(2,1)}, u32[]{:S(2)}, u32[]{:S(2)}) async-start(bf16[8,144,2048]{2,1,0:T(8,128)(2,1)} %constant_dynamic-slice_fusion), calls=%async_computation.3 | async-start | bytes 9437184 | tf_op jit(solution)/shard_map/all_to_all | solution.py:67
  44.0 0.0 all-gather.6.cloned.1.call-start
  44.1 3.5 multiply_convert_fusion.1
  47.6 0.0 all-gather.6.cloned.1.call-update
  47.7 0.0 all-gather.8.cloned.1.call-start
  47.7 0.7 all-gather.8.cloned.1.call-update
  48.4 0.0 all-gather.12.cloned.1.call-start
  48.5 100.1 %all-to-all-done.3 = bf16[8,144,2048]{2,1,0:T(8,128)(2,1)} async-done(((bf16[8,144,2048]{2,1,0:T(8,128)(2,1)}), bf16[8,144,2048]{2,1,0:T(8,128)(2,1)}, u32[]{:S(2)}, u32[]{:S(2)}) %all-to-all-start.3) | async-done | bytes 4718624 | tf_op jit(solution)/shard_map/all_to_all | solution.py:67
  148.6 0.0 all-gather.6.cloned.1.call-done
  148.6 3.6 all-to-all-start
  152.3 48.4 %all-to-all-done = bf16[8,256,512]{2,1,0:T(8,128)(2,1)S(1)} async-done(((bf16[8,256,512]{2,1,0:T(8,128)(2,1)}), bf16[8,256,512]{2,1,0:T(8,128)(2,1)S(1)}, u32[]{:S(2)}, u32[]{:S(2)}) %all-to-all-start) | async-done | bytes 2097184 | tf_op jit(solution)/shard_map/all_to_all | solution.py:37
  200.7 4.4 all-to-all-start.1
  205.0 0.0 all-gather.10.cloned.1.call-start
  205.1 2.7 convert_element_type.40
  207.8 0.0 all-gather.14.cloned.1.call-start
  207.9 1.5 copy.15
  209.4 43.4 %all-to-all-done.1 = bf16[8,256,512]{2,1,0:T(8,128)(2,1)} async-done(((bf16[8,256,512]{2,1,0:T(8,128)(2,1)}), bf16[8,256,512]{2,1,0:T(8,128)(2,1)}, u32[]{:S(2)}, u32[]{:S(2)}) %all-to-all-start.1) | async-done | bytes 2097184 | tf_op jit(solution)/shard_map/all_to_all | solution.py:38
  252.9 3.1 copy.16
  256.0 7.8 %convolution_minimum_fusion = f32[2304,512]{1,0:T(8,128)S(1)} fusion(bf16[2304,2048]{1,0:T(8,128)(2,1)} %bitcast.58, bf16[2048,512]{1,0:T(8,128)(2,1)S(1)} %bitcast.52), kind=kOutput, calls=%fused_computation.6 | convolution fusion | flops 4833017856 | bytes 16252928 | tf_op jit(solution)/shard_map/dot_general | solution.py:72
  263.8 7.3 %multiply_convert_fusion = bf16[2304,512]{1,0:T(8,128)(2,1)} fusion(f32[2304,512]{1,0:T(8,128)S(1)} %convolution_minimum_fusion, bf16[2304,2048]{1,0:T(8,128)(2,1)S(1)} %bitcast.59, bf16[2048,512]{1,0:T(8,128)(2,1)S(1)} %bitcast.54), kind=kOutput, calls=%fused_computation.7 | convolution fusion | flops 4842455040 | bytes 18612224 | tf_op jit(solution)/shard_map/dot_general | solution.py:75
  271.1 0.0 all-gather.10.cloned.1.call-done
  271.2 52.0 %all_to_all.37 = bf16[8,128,1024]{2,1,0:T(8,128)(2,1)S(1)} all-to-all(bf16[8,128,1024]{2,1,0:T(8,128)(2,1)} %all-gather.10.cloned.1.call-done), channel_id=1, replica_groups=mesh['gr'=2,'fs'=8,'tp'=2] {'fs'}, dimensions={0} | all-to-all | bytes 4194304 | tf_op jit(solution)/shard_map/all_to_all | solution.py:39
  323.2 0.2 copy.17
  323.3 0.0 all-gather.14.cloned.1.call-done
  323.4 9.9 %convolution_convert_fusion = bf16[2304,1024]{1,0:T(8,128)(2,1)} fusion(bf16[2304,1024]{1,0:T(8,128)(2,1)} %all-gather.14.cloned.1.call-done, bf16[1024,1024]{1,0:T(8,128)(2,1)S(1)} %bitcast.55), kind=kOutput, calls=%fused_computation.4 | convolution fusion | flops 4834197504 | bytes 11534336 | tf_op jit(solution)/shard_map/dot_general | solution.py:79
  333.2 4.7 %all-to-all-start.4 = ((bf16[8,288,1024]{2,1,0:T(8,128)(2,1)}), bf16[8,288,1024]{2,1,0:T(8,128)(2,1)}, u32[]{:S(2)}, u32[]{:S(2)}) async-start(bf16[8,288,1024]{2,1,0:T(8,128)(2,1)} %bitcast.50), calls=%async_computation.4 | async-start | bytes 9437184 | tf_op jit(solution)/shard_map/all_to_all | solution.py:81
  338.1 0.1 copy.21
  338.2 103.2 %all-to-all-done.4 = bf16[8,288,1024]{2,1,0:T(8,128)(2,1)} async-done(((bf16[8,288,1024]{2,1,0:T(8,128)(2,1)}), bf16[8,288,1024]{2,1,0:T(8,128)(2,1)}, u32[]{:S(2)}, u32[]{:S(2)}) %all-to-all-start.4) | async-done | bytes 4718624 | tf_op jit(solution)/shard_map/all_to_all | solution.py:81
  441.4 10.0 %gather_fusion.1 = bf16[1536,1024]{1,0:T(8,128)(2,1)S(1)} fusion(bf16[2304,1024]{1,0:T(8,128)(2,1)} %bitcast.16, s32[2048]{0:T(1024)S(1)} %pad_clamp_fusion.1), kind=kCustom, calls=%fused_computation.1 | custom fusion | bytes 6297600 | tf_op jit(solution)/shard_map/gather | solution.py:82
  451.5 4.4 reshape.127
  455.9 7.7 %multiply_reduce_fusion = bf16[384,1024]{1,0:T(8,128)(2,1)} fusion(f32[384,4,1024]{2,1,0:T(4,128)} %reshape.127, f32[384,4]{1,0:T(8,128)S(1)} %copy.21), kind=kLoop, calls=%fused_computation.3 | loop fusion | flops 2752512 | bytes 7084032 | tf_op jit(solution)/shard_map/reduce_sum | solution.py:85
  (33 shorter events, 0.3 us)
Async XLA Ops:
  7.2 13.1 %copy-start = (bf16[384,2048]{1,0:T(8,128)(2,1)S(1)}, bf16[384,2048]{1,0:T(8,128)(2,1)}, u32[]{:S(2)}) copy-start(bf16[384,2048]{1,0:T(8,128)(2,1)} %param.7) | copy-start | bytes 4718596
  36.6 7.5 %copy-start.1 = (f32[8,128,512]{2,1,0:T(8,128)S(1)}, f32[8,128,512]{2,1,0:T(8,128)}, u32[]{:S(2)}) copy-start(f32[8,128,512]{2,1,0:T(8,128)} %param.12) | copy-start | bytes 6291460
  36.6 7.5 %copy-start.6 = (f32[128]{0:T(128)S(1)}, f32[128]{0:T(128)}, u32[]{:S(2)}) copy-start(f32[128]{0:T(128)} %param.10) | copy-start | bytes 1540
  36.6 112.0 %all-to-all-start.3 = ((bf16[8,144,2048]{2,1,0:T(8,128)(2,1)}), bf16[8,144,2048]{2,1,0:T(8,128)(2,1)}, u32[]{:S(2)}, u32[]{:S(2)}) async-start(bf16[8,144,2048]{2,1,0:T(8,128)(2,1)} %constant_dynamic-slice_fusion), calls=%async_computation.3 | async-start | bytes 9437184 | tf_op jit(solution)/shard_map/all_to_all | solution.py:67
  44.0 104.6 %all-gather.6.cloned.1.call-start = ((), (), s32[]{:S(2)}) async-start(), calls=%async_computation.5 | async-start | bytes 3145728 | tf_op jit(solution)/shard_map/all_gather | solution.py:32
  47.7 104.6 %all-gather.8.cloned.1.call-start = ((), (), s32[]{:S(2)}) async-start(), calls=%async_computation.6 | async-start | bytes 3145728 | tf_op jit(solution)/shard_map/all_gather | solution.py:33
  48.4 207.5 %all-gather.12.cloned.1.call-start = ((), (), s32[]{:S(2)}) async-start(), calls=%async_computation.8 | async-start | bytes 14155776 | tf_op jit(solution)/shard_map/all_gather | solution.py:68
  148.6 52.1 %all-to-all-start = ((bf16[8,256,512]{2,1,0:T(8,128)(2,1)}), bf16[8,256,512]{2,1,0:T(8,128)(2,1)S(1)}, u32[]{:S(2)}, u32[]{:S(2)}) async-start(bf16[8,256,512]{2,1,0:T(8,128)(2,1)} %all-gather.6.cloned.1.call-done), calls=%async_computation | async-start | bytes 4194304 | tf_op jit(solution)/shard_map/all_to_all | solution.py:37
  200.7 52.2 %all-to-all-start.1 = ((bf16[8,256,512]{2,1,0:T(8,128)(2,1)}), bf16[8,256,512]{2,1,0:T(8,128)(2,1)}, u32[]{:S(2)}, u32[]{:S(2)}) async-start(bf16[8,256,512]{2,1,0:T(8,128)(2,1)} %all-gather.8.cloned.1.call-done), calls=%async_computation.1 | async-start | bytes 4194304 | tf_op jit(solution)/shard_map/all_to_all | solution.py:38
  205.0 66.1 %all-gather.10.cloned.1.call-start = ((), (), s32[]{:S(2)}) async-start(), calls=%async_computation.7 | async-start | bytes 3145728 | tf_op jit(solution)/shard_map/all_gather | solution.py:34
  207.8 115.5 %all-gather.14.cloned.1.call-start = ((), (), s32[]{:S(2)}) async-start(), calls=%async_computation.9 | async-start | bytes 7077888 | tf_op jit(solution)/shard_map/all_gather | solution.py:78
  209.4 46.5 %copy-start.2 = (bf16[1,8,2,128,512]{4,3,1,2,0:T(8,128)(2,1)S(1)}, bf16[1,8,2,128,512]{4,3,1,2,0:T(8,128)(2,1)}, u32[]{:S(2)}) copy-start(bf16[1,8,2,128,512]{4,3,1,2,0:T(8,128)(2,1)} %copy.15) | copy-start | bytes 6291460
  256.0 7.8 %copy-start.3 = (bf16[1,8,2,128,512]{4,3,1,2,0:T(8,128)(2,1)S(1)}, bf16[1,8,2,128,512]{4,3,1,2,0:T(8,128)(2,1)}, u32[]{:S(2)}) copy-start(bf16[1,8,2,128,512]{4,3,1,2,0:T(8,128)(2,1)} %copy.16) | copy-start | bytes 6291460
  256.0 7.8 %copy-start.7 = (bf16[8,288,2048]{2,1,0:T(8,128)(2,1)S(1)}, bf16[8,288,2048]{2,1,0:T(8,128)(2,1)}, u32[]{:S(2)}) copy-start(bf16[8,288,2048]{2,1,0:T(8,128)(2,1)} %all-gather.12.cloned.1.call-done) | copy-start | bytes 28311556
  323.3 9.9 %copy-start.4 = (bf16[1,8,2,64,1024]{4,3,1,2,0:T(8,128)(2,1)}, bf16[1,8,2,64,1024]{4,3,1,2,0:T(8,128)(2,1)S(1)}, u32[]{:S(2)}) copy-start(bf16[1,8,2,64,1024]{4,3,1,2,0:T(8,128)(2,1)S(1)} %copy.17) | copy-start | bytes 6291460
  333.2 4.7 %copy-start.5 = (f32[384,4]{0,1:T(4,128)S(1)}, f32[384,4]{0,1:T(4,128)}, u32[]{:S(2)}) copy-start(f32[384,4]{0,1:T(4,128)} %param.9) | copy-start | bytes 18436
  333.2 108.2 %all-to-all-start.4 = ((bf16[8,288,1024]{2,1,0:T(8,128)(2,1)}), bf16[8,288,1024]{2,1,0:T(8,128)(2,1)}, u32[]{:S(2)}, u32[]{:S(2)}) async-start(bf16[8,288,1024]{2,1,0:T(8,128)(2,1)} %bitcast.50), calls=%async_computation.4 | async-start | bytes 9437184 | tf_op jit(solution)/shard_map/all_to_all | solution.py:81
Sparse Core Ops, SparseCore 0:
  47.8 34.4 all-gather.5
  84.4 33.0 all-gather.7
  148.7 20.5 all-gather.11
  208.0 34.3 all-gather.9
  271.2 13.4 all-gather.13
where the time goes:
time: 471 us; the launch traced here: 470 us
  waiting for transfers between devices  296 us (63%)
  blocking collectives  52 us (11%)
  local copies, waits for them, and re-layouts  42.6 us (9%)
  matrix products  25 us (5%)
  starting transfers between devices  20.4 us (4%)
  other arithmetic  20.1 us (4%)
  between operations  14 us (3%)
    all_to_all x1, waiting for transfers between devices, per_device(): lax.all_to_all(answer, 'fs', split_axis=0, concat_axis=0, tiled=True)  103 us
    all_to_all x1, waiting for transfers between devices, per_device(): lax.all_to_all(mine, 'fs', split_axis=0, concat_axis=0, tiled=True)  100 us
    all_to_all x1, blocking collectives, per_device(): lax.all_to_all(paired[2], 'fs', split_axis=0, concat_axis=1, tiled=True)  52 us
    all_to_all x1, waiting for transfers between devices, per_device(): lax.all_to_all(paired[0], 'fs', split_axis=0, concat_axis=1, tiled=True)  48.4 us
    all_to_all x1, waiting for transfers between devices, per_device(): lax.all_to_all(paired[1], 'fs', split_axis=0, concat_axis=1, tiled=True)  43.4 us
    gather x1, local copies, waits for them, and re-layouts, per_device(): picked = returned.reshape(experts * capacity, returned.shape[2])[target]  10 us
    dot_general x1, matrix products, per_device(): jnp.dot(whole, w_down, preferred_element_type=jnp.float32)  9.87 us
    gather x1, local copies, waits for them, and re-layouts, per_device(): padded[anchor // per_token].reshape(experts, capacity, model_width)  9.86 us
  transfers between devices with their start and end apart: 9, of which 4 were waited for; matrix products, arithmetic and copies ran while one was open for 6% of the time, Pallas kernels for 0%

commit v1 on v0

v1 whole, which is shorter than its diff:
```python
import jax
import jax.numpy as jnp
from jax import lax
from jax.sharding import PartitionSpec as P

NORM_EPS = 1e-05
CLAMP_LIMIT = 7.0
GLU_ALPHA = 1.702


def normalize(tokens):
    values = tokens.astype(jnp.float32)
    centre = jnp.mean(values, -1, keepdims=True)
    spread = jnp.mean(jnp.square(values - centre), -1, keepdims=True)
    return ((values - centre) * lax.rsqrt(spread + NORM_EPS)).astype(jnp.bfloat16)


def dense_mixing(routes, route_scores, experts):
    mixing = jax.nn.softmax(route_scores, axis=-1)
    named = routes[:, :, None] == jnp.arange(experts, dtype=jnp.int32)[None, None, :]
    return jnp.sum(jnp.where(named, mixing[:, :, None], 0.0), axis=1)


def per_device(tokens, routes, route_scores, norm_gain, gate_master, up_master, down_master):
    experts = gate_master.shape[0]
    tok_count = tokens.shape[0]
    half = tok_count // lax.axis_size("tp")
    own_half = lax.dynamic_slice_in_dim(tokens, lax.axis_index("tp") * half, half, 0)
    rows = lax.all_gather(normalize(own_half), ("fs", "tp"), axis=0, tiled=True)
    share = dense_mixing(routes, route_scores, experts).T
    weight = lax.all_to_all(share, "fs", split_axis=0, concat_axis=0, tiled=True).reshape(-1, 1)

    def hand_over(low):
        moved = lax.all_to_all(low, "fs", split_axis=0, concat_axis=0, tiled=True)
        moved = lax.all_gather(moved, "gr", axis=0, tiled=True)
        return moved.reshape(1, moved.shape[0] * moved.shape[1], moved.shape[2])

    gate_weights = hand_over((norm_gain[None, :, None] * gate_master).astype(jnp.bfloat16))
    up_weights = hand_over((norm_gain[None, :, None] * up_master).astype(jnp.bfloat16))
    down_weights = hand_over(down_master.astype(jnp.bfloat16))
    gate_pre = jnp.minimum(
        jnp.dot(rows, gate_weights[0], preferred_element_type=jnp.float32), CLAMP_LIMIT
    )
    up_pre = jnp.clip(
        jnp.dot(rows, up_weights[0], preferred_element_type=jnp.float32), -CLAMP_LIMIT, CLAMP_LIMIT
    )
    hidden = ((up_pre + 1.0) * gate_pre * jax.nn.sigmoid(GLU_ALPHA * gate_pre)).astype(jnp.bfloat16)
    whole = lax.all_gather(hidden, "tp", axis=1, tiled=True)
    answer = jnp.dot(whole, down_weights[0], preferred_element_type=jnp.float32)
    part = (answer * weight).astype(jnp.bfloat16)
    mixed = lax.psum_scatter(part, "fs", scatter_dimension=0, tiled=True)
    return (gate_weights, up_weights, down_weights, mixed)


def solution(mesh):
    in_specs = (
        P(("gr", "fs"), None),
        P(("gr", "fs"), None),
        P(("gr", "fs"), None),
        P(("gr", "fs")),
        P(None, ("gr", "fs"), "tp"),
        P(None, ("gr", "fs"), "tp"),
        P(None, ("gr", "fs"), "tp"),
    )
    out_specs = (
        P("fs", None, "tp"),
        P("fs", None, "tp"),
        P("fs", None, "tp"),
        P(("gr", "fs"), "tp"),
    )
    return jax.shard_map(
        per_device, mesh=mesh, in_specs=in_specs, out_specs=out_specs, check_vma=False
    )
```

time: 471 us -> 421 us (0.89)
  blocking collectives: 52 us -> 123 us
  waiting for transfers between devices: 296 us -> 232 us
  local copies, waits for them, and re-layouts: 42.6 us -> 6.66 us
  starting transfers between devices: 20.4 us -> 0.25 us
  other arithmetic: 20.1 us -> 5.02 us
  matrix products: 25 us -> 39 us
    all_to_all x4 -> x0, waiting for transfers between devices: 295 us -> none  [the longest x1 103 us: per_device(): lax.all_to_all(answer, 'fs', split_axis=0, concat_axis=0, tiled=True)]
    reduce_scatter x0 -> x1, waiting for transfers between devices: none -> 119 us  [per_device(): mixed = lax.psum_scatter(part, 'fs', scatter_dimension=0, tiled=True)]
    all_gather x4, waiting for transfers between devices: 0.05 us -> 94.7 us  [the longest x1 67.6 us: per_device(): rows = lax.all_gather(normalize(own_half), ('fs', 'tp'), axis=0, tiled=True)]
    all_to_all x1 -> x4, blocking collectives: 52 us -> 123 us  [the longest x3 111 us: hand_over(): moved = lax.all_to_all(low, 'fs', split_axis=0, concat_axis=0, tiled=True)]
    all_to_all x4 -> x0, starting transfers between devices: 20.2 us -> none  [the longest x1 7.44 us: per_device(): lax.all_to_all(mine, 'fs', split_axis=0, concat_axis=0, tiled=True)]
    gather x2 -> x0, local copies, waits for them, and re-layouts: 19.9 us -> none  [the longest x1 10 us: per_device(): picked = returned.reshape(experts * capacity, returned.shape[2])[target]]
    all_gather x1, waiting for transfers between devices: 0.02 us -> 18.2 us  [per_device(): whole = lax.all_gather(hidden, 'tp', axis=1, tiled=True)]
    dot_general x3, matrix products: 25 us -> 39 us  [the longest x1 15.8 us: per_device(): jnp.dot(rows, up_weights[0], preferred_element_type=jnp.float32)]
  transfers between devices with their start and end apart: 9 -> 6, of which waited for: 4 -> 5; matrix products, arithmetic and copies ran while one was open for 6% -> 7% of each run, Pallas kernels for 0% -> 0%
where the time goes in v1:
time: 421 us
  waiting for transfers between devices  232 us (55%)
  blocking collectives  123 us (29%)
  matrix products  39 us (9%)
  between operations  14.2 us (3%)
  local copies, waits for them, and re-layouts  6.66 us (2%)
  other arithmetic  5.02 us (1%)
    reduce_scatter x1, waiting for transfers between devices, per_device(): mixed = lax.psum_scatter(part, 'fs', scatter_dimension=0, tiled=True)  119 us
    all_to_all x3, blocking collectives, hand_over(): moved = lax.all_to_all(low, 'fs', split_axis=0, concat_axis=0, tiled=True)  111 us
    all_gather x1, waiting for transfers between devices, per_device(): rows = lax.all_gather(normalize(own_half), ('fs', 'tp'), axis=0, tiled=True)  67.6 us
    all_gather x3, waiting for transfers between devices, hand_over(): moved = lax.all_gather(moved, 'gr', axis=0, tiled=True)  27 us
    all_gather x1, waiting for transfers between devices, per_device(): whole = lax.all_gather(hidden, 'tp', axis=1, tiled=True)  18.2 us
    dot_general x1, matrix products, per_device(): jnp.dot(rows, up_weights[0], preferred_element_type=jnp.float32)  15.8 us
    dot_general x1, matrix products, per_device(): jnp.dot(rows, gate_weights[0], preferred_element_type=jnp.float32)  12 us
    all_to_all x1, blocking collectives, per_device(): lax.all_to_all(share, 'fs', split_axis=0, concat_axis=0, tiled=True)  11.9 us
  transfers between devices with their start and end apart: 6, of which 5 were waited for; matrix products, arithmetic and copies ran while one was open for 7% of the time, Pallas kernels for 0%

profile of v1, /device:TPU:0, one launch (start us, length us, event | category | flops | bytes accessed | tf_op | source)
XLA Modules:
  0.0 420.6 jit_solution(722350967664827714)
XLA Ops:
  7.2 0.0 all-gather.6.cloned.1.call-start
  7.2 2.9 multiply_convert_fusion.2
  10.1 0.0 copy-start
  10.1 33.1 %all_to_all.24 = bf16[8,128,512]{2,1,0:T(8,128)(2,1)} all-to-all(bf16[8,128,512]{2,1,0:T(8,128)(2,1)S(1)} %get-tuple-element.5), channel_id=1, replica_groups=mesh['gr'=2,'fs'=8,'tp'=2] {'fs'}, dimensions={0} | all-to-all | bytes 2097152 | tf_op jit(solution)/shard_map/all_to_all | solution.py:34
  43.2 0.0 all-gather.6.cloned.1.call-update
  43.2 0.0 all-gather.12.cloned.1.call-start
  43.3 0.0 copy-done
  43.3 0.2 convert_reduce_fusion
  43.5 0.4 fusion.2
  43.9 1.4 fusion.3
  45.2 0.0 copy-start.1
  45.2 0.0 all-gather.12.cloned.1.call-update
  45.3 0.0 all-gather.8.cloned.1.call-start
  45.3 29.1 %all_to_all.25 = bf16[8,128,512]{2,1,0:T(8,128)(2,1)} all-to-all(bf16[8,128,512]{2,1,0:T(8,128)(2,1)S(1)} %get-tuple-element.4), channel_id=1, replica_groups=mesh['gr'=2,'fs'=8,'tp'=2] {'fs'}, dimensions={0} | all-to-all | bytes 2097152 | tf_op jit(solution)/shard_map/all_to_all | solution.py:34
  74.4 0.0 all-gather.8.cloned.1.call-update
  74.4 0.0 all-gather.10.cloned.1.call-start
  74.5 0.0 copy-done.1
  74.5 0.2 convert_element_type.23
  74.6 49.1 %all_to_all.26 = bf16[8,64,1024]{2,1,0:T(8,128)(2,1)} all-to-all(bf16[8,64,1024]{2,1,0:T(8,128)(2,1)S(1)} %convert_element_type.23), channel_id=1, replica_groups=mesh['gr'=2,'fs'=8,'tp'=2] {'fs'}, dimensions={0} | all-to-all | bytes 2097152 | tf_op jit(solution)/shard_map/all_to_all | solution.py:34
  123.8 0.0 all-gather.10.cloned.1.call-update
  123.8 0.0 all-gather.14.cloned.1.call-start
  123.8 0.0 all-gather.6.cloned.1.call-done
  123.9 67.6 %all-gather.12.cloned.1.call-done = bf16[3072,2048]{1,0:T(8,128)(2,1)} async-done(((bf16[192,2048]{1,0:T(8,128)(2,1)}), bf16[3072,2048]{1,0:T(8,128)(2,1)}) %all-gather.12.cloned.1.call-update) | async-done | bytes 12582928 | tf_op jit(solution)/shard_map/all_gather | solution.py:29
  191.5 12.0 %fusion.6 = f32[3072,512]{1,0:T(8,128)} fusion(bf16[3072,2048]{1,0:T(8,128)(2,1)} %all-gather.12.cloned.1.call-done, bf16[2048,512]{1,0:T(8,128)(2,1)} %bitcast.16), kind=kOutput, calls=%fused_computation.17 | convolution fusion | flops 6442450944 | bytes 20971520 | tf_op jit(solution)/shard_map/dot_general | solution.py:42
  203.5 20.9 %all-gather.8.cloned.1.call-done = bf16[16,128,512]{2,1,0:T(8,128)(2,1)} async-done(((bf16[8,128,512]{2,1,0:T(8,128)(2,1)}), bf16[16,128,512]{2,1,0:T(8,128)(2,1)}) %all-gather.8.cloned.1.call-update) | async-done | bytes 2097168 | tf_op jit(solution)/shard_map/all_gather | solution.py:35
  224.4 15.8 %multiply_convert_fusion.1 = bf16[3072,512]{1,0:T(8,128)(2,1)} fusion(f32[3072,512]{1,0:T(8,128)} %fusion.6, bf16[3072,2048]{1,0:T(8,128)(2,1)} %all-gather.12.cloned.1.call-done, bf16[2048,512]{1,0:T(8,128)(2,1)} %bitcast.18), kind=kOutput, calls=%fused_computation.1 | convolution fusion | flops 6458179584 | bytes 24117248 | tf_op jit(solution)/shard_map/dot_general | solution.py:45
  240.2 0.0 copy-start.5
  240.2 0.0 copy-start.6
  240.2 0.0 all-gather.14.cloned.1.call-update
  240.2 0.0 reduce-scatter.2.cloned.1.call-start
  240.3 0.6 copy-done.5
  241.0 0.0 copy-done.6
  241.0 11.9 %all_to_all.27 = f32[8,1,384]{2,1,0:T(1,128)S(1)} all-to-all(f32[8,1,384]{2,1,0:T(1,128)S(1)} %copy.17), channel_id=1, replica_groups=mesh['gr'=2,'fs'=8,'tp'=2] {'fs'}, dimensions={0} | all-to-all | bytes 24576 | tf_op jit(solution)/shard_map/all_to_all | solution.py:31
  252.9 6.1 %all-gather.10.cloned.1.call-done = bf16[16,64,1024]{2,1,0:T(8,128)(2,1)} async-done(((bf16[8,64,1024]{2,1,0:T(8,128)(2,1)}), bf16[16,64,1024]{2,1,0:T(8,128)(2,1)}) %all-gather.10.cloned.1.call-update) | async-done | bytes 2097168 | tf_op jit(solution)/shard_map/all_gather | solution.py:35
  258.9 18.2 %all-gather.14.cloned.1.call-done = bf16[3072,1024]{1,0:T(8,128)(2,1)} async-done(((bf16[3072,512]{1,0:T(8,128)(2,1)}), bf16[3072,1024]{1,0:T(8,128)(2,1)}) %all-gather.14.cloned.1.call-update) | async-done | bytes 6291472 | tf_op jit(solution)/shard_map/all_gather | solution.py:48
  277.1 11.3 %multiply_convert_fusion = bf16[3072,1024]{1,0:T(8,128)(2,1)} fusion(bf16[3072,1024]{1,0:T(8,128)(2,1)} %all-gather.14.cloned.1.call-done, bf16[1024,1024]{1,0:T(8,128)(2,1)} %bitcast.20, f32[3072]{0:T(1024)S(1)} %bitcast.23), kind=kOutput, calls=%fused_computation | convolution fusion | flops 6448742400 | bytes 14692352 | tf_op jit(solution)/shard_map/dot_general | solution.py:49
  288.4 0.0 copy-start.2
  288.4 0.0 reduce-scatter.2.cloned.1.call-update
  288.4 119.3 %reduce-scatter.2.cloned.1.call-done = bf16[384,1024]{1,0:T(8,128)(2,1)} async-done(((bf16[3072,1024]{1,0:T(8,128)(2,1)}), bf16[384,1024]{1,0:T(8,128)(2,1)}) %reduce-scatter.2.cloned.1.call-update) | async-done | bytes 786448 | tf_op jit(solution)/shard_map/reduce_scatter | solution.py:51
  407.8 0.0 copy-done.2
  407.8 0.0 copy-start.3
  407.8 1.3 copy.21
  409.1 1.0 copy-done.3
  410.1 0.0 copy-start.4
  410.1 1.3 copy.22
  411.4 1.0 copy-done.4
  412.5 1.3 copy.23
  (7 shorter events, 0.1 us)
Async XLA Ops:
  7.2 116.7 %all-gather.6.cloned.1.call-start = ((), (), s32[]{:S(2)}) async-start(), calls=%async_computation.5 | async-start | bytes 3145728 | tf_op jit(solution)/shard_map/all_gather | solution.py:35
  10.1 33.2 %copy-start = (bf16[384,2048]{1,0:T(8,128)(2,1)S(1)}, bf16[384,2048]{1,0:T(8,128)(2,1)}, u32[]{:S(2)}) copy-start(bf16[384,2048]{1,0:T(8,128)(2,1)} %param.7) | copy-start | bytes 4718596
  43.2 148.2 %all-gather.12.cloned.1.call-start = ((), (), s32[]{:S(2)}) async-start(), calls=%async_computation.8 | async-start | bytes 13369344 | tf_op jit(solution)/shard_map/all_gather | solution.py:29
  45.2 29.2 %copy-start.1 = (f32[8,64,1024]{2,1,0:T(8,128)S(1)}, f32[8,64,1024]{2,1,0:T(8,128)}, u32[]{:S(2)}) copy-start(f32[8,64,1024]{2,1,0:T(8,128)} %param.13) | copy-start | bytes 6291460
  45.3 179.2 %all-gather.8.cloned.1.call-start = ((), (), s32[]{:S(2)}) async-start(), calls=%async_computation.6 | async-start | bytes 3145728 | tf_op jit(solution)/shard_map/all_gather | solution.py:35
  74.4 184.5 %all-gather.10.cloned.1.call-start = ((), (), s32[]{:S(2)}) async-start(), calls=%async_computation.7 | async-start | bytes 3145728 | tf_op jit(solution)/shard_map/all_gather | solution.py:35
  123.8 153.3 %all-gather.14.cloned.1.call-start = ((), (), s32[]{:S(2)}) async-start(), calls=%async_computation.9 | async-start | bytes 9437184 | tf_op jit(solution)/shard_map/all_gather | solution.py:48
  240.2 0.7 copy-start.5
  240.2 0.8 copy-start.6
  240.2 167.5 %reduce-scatter.2.cloned.1.call-start = ((), (), s32[]{:S(2)}) async-start(), calls=%async_computation.10 | async-start | bytes 7077888 | tf_op jit(solution)/shard_map/reduce_scatter | solution.py:51
  288.4 119.4 %copy-start.2 = (bf16[16,128,512]{2,1,0:T(8,128)(2,1)S(1)}, bf16[16,128,512]{2,1,0:T(8,128)(2,1)}, u32[]{:S(2)}) copy-start(bf16[16,128,512]{2,1,0:T(8,128)(2,1)} %all-gather.6.cloned.1.call-done) | copy-start | bytes 6291460
  407.8 2.3 copy-start.3
  410.1 2.3 copy-start.4
Sparse Core Ops, SparseCore 0:
  43.4 32.0 all-gather.5
  78.4 113.0 all-gather.11
  193.0 31.3 all-gather.7
  225.8 33.0 all-gather.9
  260.3 16.7 all-gather.13
  288.5 119.1 reduce-scatter.1

commit v2 on v1

--- a/solution.py
+++ b/solution.py
@@ -1,11 +1,18 @@
+import functools
+
 import jax
 import jax.numpy as jnp
 from jax import lax
+from jax.experimental import pallas as pl
+from jax.experimental.pallas import tpu as pltpu
 from jax.sharding import PartitionSpec as P
 
 NORM_EPS = 1e-05
 CLAMP_LIMIT = 7.0
 GLU_ALPHA = 1.702
+MESH = pl.DeviceIdType.MESH
+COLUMN_TILE = 256
+VMEM_LIMIT = 56 * 1024 * 1024
 
 
 def normalize(tokens):
@@ -21,7 +28,7 @@
     return jnp.sum(jnp.where(named, mixing[:, :, None], 0.0), axis=1)
 
 
-def per_device(tokens, routes, route_scores, norm_gain, gate_master, up_master, down_master):
+def by_collectives(tokens, routes, route_scores, norm_gain, gate_master, up_master, down_master):
     experts = gate_master.shape[0]
     tok_count = tokens.shape[0]
     half = tok_count // lax.axis_size("tp")
@@ -50,6 +57,410 @@
     part = (answer * weight).astype(jnp.bfloat16)
     mixed = lax.psum_scatter(part, "fs", scatter_dimension=0, tiled=True)
     return (gate_weights, up_weights, down_weights, mixed)
+
+
+def greet(partners):
+    barrier = pltpu.get_barrier_semaphore()
+    for partner in partners:
+        pl.semaphore_signal(barrier, inc=1, device_id=partner, device_id_type=MESH)
+    pl.semaphore_wait(barrier, len(partners))
+
+
+def hand_over_kernel(
+    n_fs, gate, up, down, share, own, gate_out, up_out, down_out, share_out, rows_out,
+    kept, kept_down, kept_share, kept_rows, keep_sem,
+    out_send, out_recv, relay_send, relay_recv, share_send, share_recv,
+    line_send, line_recv, cross_send, cross_recv, twin_send, twin_recv,
+):
+    gr, fs, tp = lax.axis_index("gr"), lax.axis_index("fs"), lax.axis_index("tp")
+    n_z = n_fs // 2
+    z, y = fs // 2, fs % 2
+    lows, outs = (gate, up, down), (gate_out, up_out, down_out)
+
+    def away(dz, dy):
+        return lax.rem(z + dz, n_z) * 2 + lax.rem(y + dy, 2)
+
+    greet(
+        [{"fs": away(k // 2, k % 2)} for k in range(1, n_fs)]
+        + [{"gr": 1 - gr}, {"tp": 1 - tp}]
+    )
+
+    stays_in = [
+        pltpu.make_async_copy(gate.at[fs], kept.at[0], keep_sem.at[0]),
+        pltpu.make_async_copy(up.at[fs], kept.at[1], keep_sem.at[1]),
+        pltpu.make_async_copy(down.at[fs], kept_down, keep_sem.at[2]),
+        pltpu.make_async_copy(share.at[fs], kept_share, keep_sem.at[3]),
+        pltpu.make_async_copy(own, kept_rows, keep_sem.at[4]),
+    ]
+    stays_out = [
+        pltpu.make_async_copy(kept.at[0], gate_out.at[gr * n_fs + fs], keep_sem.at[5]),
+        pltpu.make_async_copy(kept.at[1], up_out.at[gr * n_fs + fs], keep_sem.at[6]),
+        pltpu.make_async_copy(kept_down, down_out.at[gr * n_fs + fs], keep_sem.at[7]),
+        pltpu.make_async_copy(kept_share, share_out.at[fs], keep_sem.at[8]),
+        pltpu.make_async_copy(kept_rows, rows_out.at[fs, tp], keep_sem.at[9]),
+    ]
+
+    def copy(src, dst, send, recv, partner):
+        return pltpu.make_async_remote_copy(
+            src_ref=src, dst_ref=dst, send_sem=send, recv_sem=recv,
+            device_id=partner, device_id_type=MESH,
+        )
+
+    def weight_copy(m, source, target):
+        return copy(
+            lows[m].at[target], outs[m].at[gr * n_fs + source],
+            out_send.at[m, target], out_recv.at[m, source], {"fs": target},
+        )
+
+    def relay_copy(m, source, row_of, own_input):
+        slot = outs[m].at[row_of * n_fs + source]
+        src = lows[m].at[source] if own_input else slot
+        return copy(src, slot, relay_send.at[m, source], relay_recv.at[m, source], {"gr": 1 - gr})
+
+    def share_copy(source, target):
+        return copy(
+            share.at[target], share_out.at[source],
+            share_send.at[target], share_recv.at[source], {"fs": target},
+        )
+
+    def block(zb, yb, from_own):
+        return own if from_own else rows_out.at[zb * 2 + yb, tp]
+
+    def line_copy(zb, toward, from_own):
+        way = (toward + 1) // 2
+        return copy(
+            block(zb, y, from_own), rows_out.at[zb * 2 + y, tp],
+            line_send.at[way, zb], line_recv.at[zb], {"fs": (z + toward) * 2 + y},
+        )
+
+    def cross_copy(zb, yb, from_own):
+        return copy(
+            block(zb, yb, from_own), rows_out.at[zb * 2 + yb, tp],
+            cross_send.at[zb], cross_recv.at[zb], {"fs": z * 2 + 1 - y},
+        )
+
+    def twin_copy(zb, yb, core, from_own):
+        slot = rows_out.at[zb * 2 + yb, core]
+        src = own if from_own else slot
+        return copy(
+            src, slot, twin_send.at[zb * 2 + yb], twin_recv.at[zb * 2 + yb], {"tp": 1 - tp}
+        )
+
+    def send_weights(dz):
+        for dy in range(2):
+            if dz or dy:
+                target = away(dz, dy)
+                for m in range(3):
+                    weight_copy(m, fs, target).start()
+
+    def relay(dz):
+        for dy in range(2):
+            if dz or dy:
+                source = away(n_z - dz, dy)
+                for m in range(3):
+                    weight_copy(m, source, fs).wait_recv()
+                    relay_copy(m, source, gr, False).start()
+
+    for held in stays_in:
+        held.start()
+
+    @pl.when(z > 0)
+    def _():
+        line_copy(z, -1, True).start()
+
+    @pl.when(z < n_z - 1)
+    def _():
+        line_copy(z, 1, True).start()
+
+    cross_copy(z, y, True).start()
+    twin_copy(z, y, tp, True).start()
+    for k in range(1, n_fs):
+        share_copy(fs, away(k // 2, k % 2)).start()
+    for m in range(3):
+        copy(
+            lows[m].at[fs], outs[m].at[gr * n_fs + fs],
+            relay_send.at[m, fs], relay_recv.at[m, fs], {"gr": 1 - gr},
+        ).start()
+    send_weights(0)
+    order = [d for k in range(1, n_z // 2 + 1) for d in dict.fromkeys((k, n_z - k))]
+    for held, put in zip(stays_in, stays_out):
+        held.wait()
+        put.start()
+
+    for k in range(1, n_z):
+        send_weights(order[k - 1])
+
+        @pl.when(z - k >= 0)
+        def _():
+            line_copy(z - k, 1, False).wait_recv()
+
+            @pl.when(z < n_z - 1)
+            def _():
+                line_copy(z - k, 1, False).start()
+
+            cross_copy(z - k, y, False).start()
+            twin_copy(z - k, y, tp, False).start()
+
+        @pl.when(z + k < n_z)
+        def _():
+            line_copy(z + k, -1, False).wait_recv()
+
+            @pl.when(z > 0)
+            def _():
+                line_copy(z + k, -1, False).start()
+
+            cross_copy(z + k, y, False).start()
+            twin_copy(z + k, y, tp, False).start()
+
+        relay(0 if k == 1 else order[k - 2])
+
+    def crossed(zb):
+        cross_copy(zb, 1 - y, False).wait_recv()
+        twin_copy(zb, 1 - y, tp, False).start()
+
+    for zb in range(n_z):
+        crossed(zb)
+    relay(order[n_z - 2])
+
+    for zb in range(n_z):
+        @pl.when(z > 0)
+        def _():
+            @pl.when(zb >= z)
+            def _():
+                line_copy(zb, -1, False).wait_send()
+
+        @pl.when(z < n_z - 1)
+        def _():
+            @pl.when(zb <= z)
+            def _():
+                line_copy(zb, 1, False).wait_send()
+
+        cross_copy(zb, y, False).wait_send()
+    for k in range(n_fs):
+        twin_copy(k // 2, k % 2, tp, False).wait_send()
+        twin_copy(k // 2, k % 2, 1 - tp, False).wait_recv()
+    for k in range(1, n_fs):
+        other = away(k // 2, k % 2)
+        share_copy(fs, other).wait_send()
+        share_copy(other, fs).wait_recv()
+        for m in range(3):
+            weight_copy(m, fs, other).wait_send()
+    for k in range(n_fs):
+        for m in range(3):
+            relay_copy(m, k, gr, False).wait_send()
+            relay_copy(m, k, 1 - gr, False).wait_recv()
+    for put in stays_out:
+        put.wait()
+
+
+def hand_over(gate_low, up_low, down_low, share, own):
+    n_fs, n_gr, n_tp = (lax.axis_size(axis) for axis in ("fs", "gr", "tp"))
+    half, width = own.shape
+    like = jax.ShapeDtypeStruct
+    dma = pltpu.SemaphoreType.DMA
+    outs = [like((n_gr * n_fs,) + low.shape[1:], low.dtype) for low in (gate_low, up_low, down_low)]
+    outs += [like(share.shape, share.dtype), like((n_fs, n_tp, half, width), own.dtype)]
+    return pl.pallas_call(
+        functools.partial(hand_over_kernel, n_fs),
+        out_shape=outs,
+        in_specs=[pl.BlockSpec(memory_space=pl.ANY)] * 5,
+        out_specs=[pl.BlockSpec(memory_space=pl.ANY)] * 5,
+        scratch_shapes=[
+            pltpu.VMEM((2,) + gate_low.shape[1:], gate_low.dtype),
+            pltpu.VMEM(down_low.shape[1:], down_low.dtype),
+            pltpu.VMEM(share.shape[1:], share.dtype),
+            pltpu.VMEM(own.shape, own.dtype),
+            dma((10,)),
+            dma((3, n_fs)), dma((3, n_fs)), dma((3, n_fs)), dma((3, n_fs)),
+            dma((n_fs,)), dma((n_fs,)),
+            dma((2, n_fs // 2)), dma((n_fs // 2,)),
+            dma((n_fs // 2,)), dma((n_fs // 2,)),
+            dma((n_fs,)), dma((n_fs,)),
+        ],
+        compiler_params=pltpu.CompilerParams(
+            collective_id=0, has_side_effects=True, vmem_limit_bytes=VMEM_LIMIT
+        ),
+    )(gate_low, up_low, down_low, share, own)
+
+
+def experts_kernel(
+    n_fs, rows, gate, up, down, weight, out,
+    hid_own, hid_got, ysend, ygot, zsend, zgot,
+    hid_send, hid_recv, y_send, y_recv, z_send, z_recv,
+):
+    fs, tp = lax.axis_index("fs"), lax.axis_index("tp")
+    n_z = n_fs // 2
+    z, y = fs // 2, fs % 2
+    hid_cols, out_cols = gate.shape[1], down.shape[1]
+    greet(
+        [{"fs": lax.rem(z + k, n_z) * 2 + y} for k in range(1, n_z)]
+        + [{"fs": z * 2 + 1 - y}, {"tp": 1 - tp}]
+    )
+
+    def copy(src, dst, send, recv, partner):
+        return pltpu.make_async_remote_copy(
+            src_ref=src, dst_ref=dst, send_sem=send, recv_sem=recv,
+            device_id=partner, device_id_type=MESH,
+        )
+
+    def hid_copy(j):
+        return copy(
+            hid_own.at[j], hid_got.at[j], hid_send.at[j], hid_recv.at[j], {"tp": 1 - tp}
+        )
+
+    def y_copy(i):
+        return copy(ysend.at[i], ygot.at[i], y_send.at[i], y_recv.at[i], {"fs": z * 2 + 1 - y})
+
+    def z_copy(i):
+        target = lax.rem(z + n_z - 1 - i, n_z) * 2 + y
+        return copy(zsend.at[i], zgot.at[i], z_send.at[i], z_recv.at[i], {"fs": target})
+
+    def target_of(j):
+        phase, i = j // n_z, j % n_z
+        return lax.rem(z + n_z - 1 - i, n_z) * 2 + lax.rem(y + 1 + phase, 2)
+
+    def fill_hidden(j):
+        block = target_of(j)
+
+        @pl.loop(0, hid_cols // COLUMN_TILE)
+        def _(c):
+            cols = pl.ds(pl.multiple_of(c * COLUMN_TILE, COLUMN_TILE), COLUMN_TILE)
+            gate_pre = jnp.minimum(
+                jnp.dot(rows[block], gate[:, cols], preferred_element_type=jnp.float32),
+                CLAMP_LIMIT,
+            )
+            up_pre = jnp.clip(
+                jnp.dot(rows[block], up[:, cols], preferred_element_type=jnp.float32),
+                -CLAMP_LIMIT,
+                CLAMP_LIMIT,
+            )
+            hidden = (up_pre + 1.0) * gate_pre * jax.nn.sigmoid(GLU_ALPHA * gate_pre)
+            hid_own[j, :, cols] = hidden.astype(jnp.bfloat16)
+
+        hid_copy(j).start()
+
+    def weighted(j, cols):
+        mine = pl.ds(pl.multiple_of(tp * hid_cols, hid_cols), hid_cols)
+        theirs = pl.ds(pl.multiple_of((1 - tp) * hid_cols, hid_cols), hid_cols)
+        answer = jnp.dot(hid_own[j], down[mine, cols], preferred_element_type=jnp.float32)
+        answer += jnp.dot(hid_got[j], down[theirs, cols], preferred_element_type=jnp.float32)
+        return answer * weight[target_of(j)]
+
+    def tiles(body):
+        @pl.loop(0, out_cols // COLUMN_TILE)
+        def _(c):
+            body(pl.ds(pl.multiple_of(c * COLUMN_TILE, COLUMN_TILE), COLUMN_TILE))
+
+    fill_hidden(0)
+
+    @pl.loop(0, n_fs)
+    def _(p):
+        @pl.when(p < n_fs - 1)
+        def _():
+            fill_hidden(p + 1)
+
+        hid_copy(p).wait_recv()
+
+        @pl.when(p < n_z)
+        def _():
+            def body(cols):
+                ysend[p, :, cols] = weighted(p, cols).astype(jnp.bfloat16)
+
+            tiles(body)
+            y_copy(p).start()
+
+        @pl.when(p >= n_z)
+        def _():
+            i = p - n_z
+            y_copy(i).wait_recv()
+
+            def body(cols):
+                total = weighted(p, cols) + ygot[i, :, cols].astype(jnp.float32)
+                zsend[i, :, cols] = total.astype(jnp.bfloat16)
+
+            tiles(body)
+
+            @pl.when(i < n_z - 1)
+            def _():
+                z_copy(i).start()
+
+    for i in range(n_z - 1):
+        z_copy(i).wait_recv()
+
+    def close(cols):
+        total = zsend[n_z - 1, :, cols].astype(jnp.float32)
+        for i in range(n_z - 1):
+            total += zgot[i, :, cols].astype(jnp.float32)
+        out[:, cols] = total.astype(jnp.bfloat16)
+
+    tiles(close)
+    for j in range(n_fs):
+        hid_copy(j).wait_send()
+    for i in range(n_z):
+        y_copy(i).wait_send()
+    for i in range(n_z - 1):
+        z_copy(i).wait_send()
+
+
+def experts_here(rows, gate, up, down, weight):
+    n_fs, tok_count, width = rows.shape
+    n_z = n_fs // 2
+    hid_cols, out_cols = gate.shape[1], down.shape[1]
+    dma = pltpu.SemaphoreType.DMA
+    low = jnp.bfloat16
+    return pl.pallas_call(
+        functools.partial(experts_kernel, n_fs),
+        out_shape=jax.ShapeDtypeStruct((tok_count, out_cols), low),
+        in_specs=[pl.BlockSpec(memory_space=pltpu.VMEM)] * 5,
+        out_specs=pl.BlockSpec(memory_space=pltpu.VMEM),
+        scratch_shapes=[
+            pltpu.VMEM((n_fs, tok_count, hid_cols), low),
+            pltpu.VMEM((n_fs, tok_count, hid_cols), low),
+            pltpu.VMEM((n_z, tok_count, out_cols), low),
+            pltpu.VMEM((n_z, tok_count, out_cols), low),
+            pltpu.VMEM((n_z, tok_count, out_cols), low),
+            pltpu.VMEM((n_z - 1, tok_count, out_cols), low),
+            dma((n_fs,)), dma((n_fs,)),
+            dma((n_z,)), dma((n_z,)),
+            dma((n_z - 1,)), dma((n_z - 1,)),
+        ],
+        compiler_params=pltpu.CompilerParams(
+            collective_id=1, has_side_effects=True, vmem_limit_bytes=VMEM_LIMIT
+        ),
+    )(rows, gate, up, down, weight)
+
+
+def fits_in_kernels(tokens, gate_master):
+    n_fs, n_gr, n_tp = (lax.axis_size(axis) for axis in ("fs", "gr", "tp"))
+    tok_count, width = tokens.shape
+    held = 2 * n_fs * tok_count * (width + 5 * gate_master.shape[2])
+    return n_fs % 2 == 0 and n_gr == 2 and n_tp == 2 and held < VMEM_LIMIT * 3 // 4
+
+
+def per_device(tokens, routes, route_scores, norm_gain, gate_master, up_master, down_master):
+    if not fits_in_kernels(tokens, gate_master):
+        return by_collectives(
+            tokens, routes, route_scores, norm_gain, gate_master, up_master, down_master
+        )
+    experts, n_fs = gate_master.shape[0], lax.axis_size("fs")
+    tok_count, width = tokens.shape
+    half = tok_count // lax.axis_size("tp")
+    own = normalize(lax.dynamic_slice_in_dim(tokens, lax.axis_index("tp") * half, half, 0))
+    share = dense_mixing(routes, route_scores, experts).T.reshape(experts, 1, tok_count)
+    gate, up, down, weight, rows = hand_over(
+        (norm_gain[None, :, None] * gate_master).astype(jnp.bfloat16),
+        (norm_gain[None, :, None] * up_master).astype(jnp.bfloat16),
+        down_master.astype(jnp.bfloat16),
+        share,
+        own,
+    )
+    gate = gate.reshape(-1, gate.shape[2])
+    up = up.reshape(-1, up.shape[2])
+    down = down.reshape(-1, down.shape[2])
+    mixed = experts_here(
+        rows.reshape(n_fs, tok_count, width), gate, up, down, weight.reshape(n_fs, tok_count, 1)
+    )
+    return (gate[None], up[None], down[None], mixed)
 
 
 def solution(mesh):

time: 421 us -> 292 us (0.69)
  Pallas kernels: 0 us -> 269 us
  waiting for transfers between devices: 232 us -> 0 us
  blocking collectives: 123 us -> 0 us
  matrix products: 39 us -> 0 us
  between operations: 14.2 us -> 0.7 us
  other arithmetic: 5.02 us -> 12.8 us
    pallas_call x0 -> x2, Pallas kernels: none -> 269 us  [the longest x1 140 us: hand_over(): pl.pallas_call(functools.partial(hand_over_kernel, n_fs), out_shape=outs,...]
    all_to_all x4 -> x0, blocking collectives: 123 us -> none  [the longest x3 111 us: hand_over(): moved = lax.all_to_all(low, 'fs', split_axis=0, concat_axis=0, tiled=True)]
    reduce_scatter x1 -> x0, waiting for transfers between devices: 119 us -> none  [per_device(): mixed = lax.psum_scatter(part, 'fs', scatter_dimension=0, tiled=True)]
    all_gather x5 -> x0, waiting for transfers between devices: 113 us -> none  [the longest x1 67.6 us: per_device(): rows = lax.all_gather(normalize(own_half), ('fs', 'tp'), axis=0, tiled=True)]
    dot_general x3 -> x0, matrix products: 39 us -> none  [the longest x1 15.8 us: per_device(): jnp.dot(rows, up_weights[0], preferred_element_type=jnp.float32)]
  transfers between devices with their start and end apart: 6 -> 0, of which waited for: 5 -> 0; matrix products, arithmetic and copies ran while one was open for 7% -> 0% of each run, Pallas kernels for 0% -> 0%
where the time goes in v2:
time: 292 us
  Pallas kernels  269 us (92%)
  other arithmetic  12.8 us (4%)
  local copies, waits for them, and re-layouts  9.48 us (3%)
    pallas_call x1, Pallas kernels, hand_over(): pl.pallas_call(functools.partial(hand_over_kernel, n_fs), out_shape=outs,...  140 us
    pallas_call x1, Pallas kernels, experts_here(): pl.pallas_call(functools.partial(experts_kernel, n_fs), out_shape=jax.Sha...  129 us
    unnamed x20, local copies, waits for them, and re-layouts  7.26 us

profile of v2, /device:TPU:0, one launch (start us, length us, event | category | flops | bytes accessed | tf_op | source)
XLA Modules:
  0.0 291.9 jit_solution(3973044641193398590)
XLA Ops:
  0.6 0.0 copy-start.3
  0.6 1.4 convert_reduce_fusion
  2.1 1.5 fusion.2
  3.6 0.7 reduce_max.9
  4.3 0.7 fusion.5
  5.0 0.7 fusion.4
  5.7 0.7 select_reduce_fusion
  6.4 0.6 reshape.43.share
  7.0 0.0 copy-done.3
  7.0 0.0 copy-start.5
  7.0 0.0 copy-start.6
  7.0 0.0 copy-start.7
  7.1 1.3 fusion.3.own
  8.4 2.9 %convert_element_type.17.down = bf16[8,64,1024]{2,1,0:T(8,128)(2,1)} convert(f32[8,64,1024]{2,1,0:T(8,128)} %param.13) | non-fusion elementwise | flops 524288 | bytes 3145728 | tf_op jit(solution)/shard_map/convert_element_type | solution.py:453
  11.3 0.0 copy-done.5
  11.3 0.0 copy-done.6
  11.3 0.0 copy-done.7
  11.3 2.0 multiply_convert_fusion
  13.4 139.7 %shard_map.102 = (bf16[16,128,512]{2,1,0:T(8,128)(2,1)}, bf16[16,128,512]{2,1,0:T(8,128)(2,1)}, bf16[16,64,1024]{2,1,0:T(8,128)(2,1)}, f32[8,1,384]{2,1,0:T(1,128)}, bf16[8,2,192,2048]{3,2,1,0:T(8,128)(2,1)}) custom-call(bf16[8,128,512]{2,1,0:T(8,128)(2,1)} %get-tuple-element.15.gate, bf16[8,128,512]{2,1,0:T(8,128)(2,1)} %get-tuple-element.14.up, ...), custom_call_target="tpu_custom_call" | custom-call | tf_op jit(solution)/shard_map/pallas_call | solution.py:263
  153.0 0.7 reduce
  153.8 1.6 reshape.49.weight
  155.4 0.0 copy-start.2
  155.4 129.2 %shard_map.103 = bf16[384,1024]{1,0:T(8,128)(2,1)} custom-call(bf16[8,384,2048]{2,1,0:T(8,128)(2,1)} %bitcast.8, bf16[2048,512]{1,0:T(8,128)(2,1)} %bitcast.13, bf16[2048,512]{1,0:T(8,128)(2,1)} %bitcast.11, bf16[1024,1024]{1,0:T(8,128)(2,1)} %bitcast.9, f32[8,384,1]{2,1,0:T(8,128)} %reshape.49.weight), custom_call_target="tpu_custom_call" | custom-call | tf_op jit(solution)/shard_map/pallas_call | solution.py:411
  284.6 0.0 copy-done.2
  284.7 0.0 copy-start.1
  284.7 1.3 copy.21
  286.0 1.0 copy-done.1
  287.0 0.0 copy-start
  287.0 1.3 copy.22
  288.3 1.0 copy-done
  289.3 0.0 copy-start.4
  289.4 1.3 copy.23
  290.7 0.4 copy-done.4
  291.0 0.9 copy.24
  (2 shorter events, 0.0 us)
Async XLA Ops:
  0.6 6.4 %copy-start.3 = (bf16[384,2048]{1,0:T(8,128)(2,1)S(1)}, bf16[384,2048]{1,0:T(8,128)(2,1)}, u32[]{:S(2)}) copy-start(bf16[384,2048]{1,0:T(8,128)(2,1)} %param.7) | copy-start | bytes 4718596
  7.0 4.3 %copy-start.5 = (f32[8,128,512]{2,1,0:T(8,128)S(1)}, f32[8,128,512]{2,1,0:T(8,128)}, u32[]{:S(2)}) copy-start(f32[8,128,512]{2,1,0:T(8,128)} %param.12) | copy-start | bytes 6291460
  7.0 4.3 %copy-start.6 = (f32[8,128,512]{2,1,0:T(8,128)S(1)}, f32[8,128,512]{2,1,0:T(8,128)}, u32[]{:S(2)}) copy-start(f32[8,128,512]{2,1,0:T(8,128)} %param.11) | copy-start | bytes 6291460
  7.0 4.3 %copy-start.7 = (f32[128]{0:T(128)S(1)}, f32[128]{0:T(128)}, u32[]{:S(2)}) copy-start(f32[128]{0:T(128)} %param.10) | copy-start | bytes 1540
  155.4 129.2 %copy-start.2 = (bf16[16,128,512]{2,1,0:T(8,128)(2,1)S(1)}, bf16[16,128,512]{2,1,0:T(8,128)(2,1)}, u32[]{:S(2)}) copy-start(bf16[16,128,512]{2,1,0:T(8,128)(2,1)} %get-tuple-element.9) | copy-start | bytes 6291460
  284.7 2.3 copy-start.1
  287.0 2.3 copy-start
  289.3 1.7 copy-start.4

commit v3 on v2

--- a/solution.py
+++ b/solution.py
@@ -218,9 +218,9 @@
         cross_copy(zb, 1 - y, False).wait_recv()
         twin_copy(zb, 1 - y, tp, False).start()
 
+    relay(order[n_z - 2])
     for zb in range(n_z):
         crossed(zb)
-    relay(order[n_z - 2])
 
     for zb in range(n_z):
         @pl.when(z > 0)
@@ -308,15 +308,25 @@
             hid_own.at[j], hid_got.at[j], hid_send.at[j], hid_recv.at[j], {"tp": 1 - tp}
         )
 
-    def y_copy(i):
-        return copy(ysend.at[i], ygot.at[i], y_send.at[i], y_recv.at[i], {"fs": z * 2 + 1 - y})
-
-    def z_copy(i):
+    def y_copy(i, c):
+        return copy(
+            ysend.at[i, c], ygot.at[i, c], y_send.at[i, c], y_recv.at[i, c],
+            {"fs": z * 2 + 1 - y},
+        )
+
+    def z_copy(i, c):
         target = lax.rem(z + n_z - 1 - i, n_z) * 2 + y
-        return copy(zsend.at[i], zgot.at[i], z_send.at[i], z_recv.at[i], {"fs": target})
+        return copy(
+            zsend.at[i, c], zgot.at[i, c], z_send.at[i, c], z_recv.at[i, c], {"fs": target}
+        )
+
+    def place(j):
+        last = j // (n_fs - 1)
+        phase = ((j + 1) % 2) * ((j + n_fs - 1) // n_fs) + last
+        return phase, (1 - phase) * ((j + 1) // 2) + phase * (j // 2 - 1 + last)
 
     def target_of(j):
-        phase, i = j // n_z, j % n_z
+        phase, i = place(j)
         return lax.rem(z + n_z - 1 - i, n_z) * 2 + lax.rem(y + 1 + phase, 2)
 
     def fill_hidden(j):
@@ -346,10 +356,12 @@
         answer += jnp.dot(hid_got[j], down[theirs, cols], preferred_element_type=jnp.float32)
         return answer * weight[target_of(j)]
 
+    count = out_cols // COLUMN_TILE
+
     def tiles(body):
-        @pl.loop(0, out_cols // COLUMN_TILE)
+        @pl.loop(0, count)
         def _(c):
-            body(pl.ds(pl.multiple_of(c * COLUMN_TILE, COLUMN_TILE), COLUMN_TILE))
+            body(c, pl.ds(pl.multiple_of(c * COLUMN_TILE, COLUMN_TILE), COLUMN_TILE))
 
     fill_hidden(0)
 
@@ -361,51 +373,53 @@
 
         hid_copy(p).wait_recv()
 
-        @pl.when(p < n_z)
-        def _():
-            def body(cols):
-                ysend[p, :, cols] = weighted(p, cols).astype(jnp.bfloat16)
+        phase, i = place(p)
+
+        @pl.when(phase == 0)
+        def _():
+            def body(c, cols):
+                ysend[i, c] = weighted(p, cols).astype(jnp.bfloat16)
+                y_copy(i, c).start()
 
             tiles(body)
-            y_copy(p).start()
-
-        @pl.when(p >= n_z)
-        def _():
-            i = p - n_z
-            y_copy(i).wait_recv()
-
-            def body(cols):
-                total = weighted(p, cols) + ygot[i, :, cols].astype(jnp.float32)
-                zsend[i, :, cols] = total.astype(jnp.bfloat16)
+
+        @pl.when(phase == 1)
+        def _():
+            def body(c, cols):
+                y_copy(i, c).wait_recv()
+                total = weighted(p, cols) + ygot[i, c].astype(jnp.float32)
+                zsend[i, c] = total.astype(jnp.bfloat16)
+
+                @pl.when(i < n_z - 1)
+                def _():
+                    z_copy(i, c).start()
 
             tiles(body)
 
-            @pl.when(i < n_z - 1)
-            def _():
-                z_copy(i).start()
-
-    for i in range(n_z - 1):
-        z_copy(i).wait_recv()
-
-    def close(cols):
-        total = zsend[n_z - 1, :, cols].astype(jnp.float32)
+    def close(c, cols):
+        total = zsend[n_z - 1, c].astype(jnp.float32)
         for i in range(n_z - 1):
-            total += zgot[i, :, cols].astype(jnp.float32)
+            z_copy(i, c).wait_recv()
+            total += zgot[i, c].astype(jnp.float32)
         out[:, cols] = total.astype(jnp.bfloat16)
 
     tiles(close)
     for j in range(n_fs):
         hid_copy(j).wait_send()
-    for i in range(n_z):
-        y_copy(i).wait_send()
-    for i in range(n_z - 1):
-        z_copy(i).wait_send()
+
+    @pl.loop(0, count)
+    def _(c):
+        for i in range(n_z):
+            y_copy(i, c).wait_send()
+        for i in range(n_z - 1):
+            z_copy(i, c).wait_send()
 
 
 def experts_here(rows, gate, up, down, weight):
     n_fs, tok_count, width = rows.shape
     n_z = n_fs // 2
     hid_cols, out_cols = gate.shape[1], down.shape[1]
+    count = out_cols // COLUMN_TILE
     dma = pltpu.SemaphoreType.DMA
     low = jnp.bfloat16
     return pl.pallas_call(
@@ -416,13 +430,13 @@
         scratch_shapes=[
             pltpu.VMEM((n_fs, tok_count, hid_cols), low),
             pltpu.VMEM((n_fs, tok_count, hid_cols), low),
-            pltpu.VMEM((n_z, tok_count, out_cols), low),
-            pltpu.VMEM((n_z, tok_count, out_cols), low),
-            pltpu.VMEM((n_z, tok_count, out_cols), low),
-            pltpu.VMEM((n_z - 1, tok_count, out_cols), low),
+            pltpu.VMEM((n_z, count, tok_count, COLUMN_TILE), low),
+            pltpu.VMEM((n_z, count, tok_count, COLUMN_TILE), low),
+            pltpu.VMEM((n_z, count, tok_count, COLUMN_TILE), low),
+            pltpu.VMEM((n_z - 1, count, tok_count, COLUMN_TILE), low),
             dma((n_fs,)), dma((n_fs,)),
-            dma((n_z,)), dma((n_z,)),
-            dma((n_z - 1,)), dma((n_z - 1,)),
+            dma((n_z, count)), dma((n_z, count)),
+            dma((n_z - 1, count)), dma((n_z - 1, count)),
         ],
         compiler_params=pltpu.CompilerParams(
             collective_id=1, has_side_effects=True, vmem_limit_bytes=VMEM_LIMIT

time: 292 us -> 278 us (0.952)
  Pallas kernels: 269 us -> 254 us
    pallas_call x1, Pallas kernels: 140 us -> 130 us  [hand_over(): pl.pallas_call(functools.partial(hand_over_kernel, n_fs), out_shape=outs,...]
    pallas_call x1, Pallas kernels: 129 us -> 124 us  [experts_here(): pl.pallas_call(functools.partial(experts_kernel, n_fs), out_shape=jax.Sha...]
where the time goes in v3:
time: 278 us; the launch traced here: 277 us
  Pallas kernels  254 us (91%)
  other arithmetic  12.8 us (5%)
  local copies, waits for them, and re-layouts  9.48 us (3%)
    pallas_call x1, Pallas kernels, hand_over(): pl.pallas_call(functools.partial(hand_over_kernel, n_fs), out_shape=outs,...  130 us
    pallas_call x1, Pallas kernels, experts_here(): pl.pallas_call(functools.partial(experts_kernel, n_fs), out_shape=jax.Sha...  124 us
    unnamed x20, local copies, waits for them, and re-layouts  7.26 us

profile of v3, /device:TPU:0, one launch (start us, length us, event | category | flops | bytes accessed | tf_op | source)
XLA Modules:
  0.0 277.3 jit_solution(12532949964288509164)
XLA Ops:
  0.6 0.0 copy-start.3
  0.6 1.4 convert_reduce_fusion
  2.1 1.5 fusion.2
  3.6 0.7 reduce_max.9
  4.3 0.7 fusion.5
  5.0 0.7 fusion.4
  5.7 0.7 select_reduce_fusion
  6.4 0.6 reshape.43.share
  7.0 0.0 copy-done.3
  7.0 0.0 copy-start.5
  7.0 0.0 copy-start.6
  7.0 0.0 copy-start.7
  7.1 1.3 fusion.3.own
  8.4 2.9 %convert_element_type.17.down = bf16[8,64,1024]{2,1,0:T(8,128)(2,1)} convert(f32[8,64,1024]{2,1,0:T(8,128)} %param.13) | non-fusion elementwise | flops 524288 | bytes 3145728 | tf_op jit(solution)/shard_map/convert_element_type | solution.py:467
  11.3 0.0 copy-done.5
  11.3 0.0 copy-done.6
  11.3 0.0 copy-done.7
  11.3 2.0 multiply_convert_fusion
  13.4 129.8 %shard_map.102 = (bf16[16,128,512]{2,1,0:T(8,128)(2,1)}, bf16[16,128,512]{2,1,0:T(8,128)(2,1)}, bf16[16,64,1024]{2,1,0:T(8,128)(2,1)}, f32[8,1,384]{2,1,0:T(1,128)}, bf16[8,2,192,2048]{3,2,1,0:T(8,128)(2,1)}) custom-call(bf16[8,128,512]{2,1,0:T(8,128)(2,1)} %get-tuple-element.15.gate, bf16[8,128,512]{2,1,0:T(8,128)(2,1)} %get-tuple-element.14.up, ...), custom_call_target="tpu_custom_call" | custom-call | tf_op jit(solution)/shard_map/pallas_call | solution.py:263
  143.2 0.7 reduce
  144.0 1.6 reshape.49.weight
  145.6 0.0 copy-start.2
  145.6 124.5 %shard_map.103 = bf16[384,1024]{1,0:T(8,128)(2,1)} custom-call(bf16[8,384,2048]{2,1,0:T(8,128)(2,1)} %bitcast.8, bf16[2048,512]{1,0:T(8,128)(2,1)} %bitcast.13, bf16[2048,512]{1,0:T(8,128)(2,1)} %bitcast.11, bf16[1024,1024]{1,0:T(8,128)(2,1)} %bitcast.9, f32[8,384,1]{2,1,0:T(8,128)} %reshape.49.weight), custom_call_target="tpu_custom_call" | custom-call | tf_op jit(solution)/shard_map/pallas_call | solution.py:425
  270.0 0.0 copy-done.2
  270.0 0.0 copy-start.1
  270.1 1.3 copy.21
  271.4 1.0 copy-done.1
  272.4 0.0 copy-start
  272.4 1.3 copy.22
  273.7 1.0 copy-done
  274.7 0.0 copy-start.4
  274.7 1.3 copy.23
  276.1 0.4 copy-done.4
  276.4 0.9 copy.24
  (2 shorter events, 0.0 us)
Async XLA Ops:
  0.6 6.4 %copy-start.3 = (bf16[384,2048]{1,0:T(8,128)(2,1)S(1)}, bf16[384,2048]{1,0:T(8,128)(2,1)}, u32[]{:S(2)}) copy-start(bf16[384,2048]{1,0:T(8,128)(2,1)} %param.7) | copy-start | bytes 4718596
  7.0 4.3 %copy-start.5 = (f32[8,128,512]{2,1,0:T(8,128)S(1)}, f32[8,128,512]{2,1,0:T(8,128)}, u32[]{:S(2)}) copy-start(f32[8,128,512]{2,1,0:T(8,128)} %param.12) | copy-start | bytes 6291460
  7.0 4.3 %copy-start.6 = (f32[8,128,512]{2,1,0:T(8,128)S(1)}, f32[8,128,512]{2,1,0:T(8,128)}, u32[]{:S(2)}) copy-start(f32[8,128,512]{2,1,0:T(8,128)} %param.11) | copy-start | bytes 6291460
  7.0 4.3 %copy-start.7 = (f32[128]{0:T(128)S(1)}, f32[128]{0:T(128)}, u32[]{:S(2)}) copy-start(f32[128]{0:T(128)} %param.10) | copy-start | bytes 1540
  145.6 124.5 %copy-start.2 = (bf16[16,128,512]{2,1,0:T(8,128)(2,1)S(1)}, bf16[16,128,512]{2,1,0:T(8,128)(2,1)}, u32[]{:S(2)}) copy-start(bf16[16,128,512]{2,1,0:T(8,128)(2,1)} %get-tuple-element.9) | copy-start | bytes 6291460
  270.0 2.3 copy-start.1
  272.4 2.3 copy-start
  274.7 1.7 copy-start.4
